TPU v7x, 32 devices: a whole 2x2x4 slice. The times are simulated.
32 devices in a mesh: fs: 16 (over z, y, x), tp: 2 (over core).
Axes of the slice: x: 2, y: 2, z: 4, core: 2. Of those that a mesh axis runs over, the one named last changes fastest.
Arguments:
- tokens: bfloat16 [6144, 2048], P('fs'), may hold values from -6 to 6
- mixer_norm_gain: float32 [2048], replicated, may hold values from 0.1 to 1.9
- outer_gate_weight: bfloat16 [2048, 2048], P('fs', 'tp'), may hold values from -0.125 to 0.125
- inner_gate_weight: bfloat16 [2048, 2048], P('fs', 'tp'), may hold values from -0.125 to 0.125
- value_projection_weight: bfloat16 [2048, 2048], P('fs', 'tp'), may hold values from -0.125 to 0.125
- filter_taps_weight: float32 [3, 2048], replicated, may hold values from -3 to 3
- mixer_output_weight: bfloat16 [2048, 2048], P('tp', 'fs'), may hold values from -0.125 to 0.125
- feedforward_norm_gain: float32 [2048], replicated, may hold values from 0.1 to 1.9
- up_projection_weight: bfloat16 [2048, 8192], P('fs', 'tp'), may hold values from -0.125 to 0.125
- down_projection_weight: bfloat16 [8192, 2048], P('tp', 'fs'), may hold values from -0.0625 to 0.0625
Outputs:
- layer_out: bfloat16 [6144, 2048], P('fs')
All inputs are finite; a program needn't handle non-finite values.
Results may differ from a plain program's by a relative error of at most 0.02.
Values may be sent and summed in bfloat16 or wider, within the bound.
A program may use at most 128 MiB of HBM per device.

v0:
```python
import jax
import jax.numpy as jnp
from jax import lax
from jax.sharding import PartitionSpec as P


def rms_norm(rows, gain):
    floats = rows.astype(jnp.float32)
    scale = lax.rsqrt(jnp.mean(floats * floats, axis=-1, keepdims=True) + 1e-06)
    return (floats * scale * gain).astype(jnp.bfloat16)


def causal_mix(inner_product_rows, taps):
    length = inner_product_rows.shape[0]
    width = taps.shape[0]
    padded = jnp.pad(inner_product_rows, ((width - 1, 0), (0, 0)))
    total = jnp.zeros_like(inner_product_rows)
    for offset in range(width):
        total = total + taps[offset] * padded[offset : offset + length]
    return total


def settle(partial_value):
    rounded = lax.optimization_barrier(partial_value.astype(jnp.bfloat16))
    return rounded.astype(jnp.float32)


def on_device(
    tokens,
    mixer_norm_gain,
    outer_gate_weight,
    inner_gate_weight,
    value_projection_weight,
    filter_taps_weight,
    mixer_output_weight,
    feedforward_norm_gain,
    up_projection_weight,
    down_projection_weight,
):
    index = lax.axis_index("tp")
    local_width = outer_gate_weight.shape[1]
    first_normed_rows = rms_norm(tokens, mixer_norm_gain)
    pieces = (
        lax.all_gather(outer_gate_weight, "fs", axis=0, tiled=True),
        lax.all_gather(inner_gate_weight, "fs", axis=0, tiled=True),
        lax.all_gather(value_projection_weight, "fs", axis=0, tiled=True),
    )
    columns = first_normed_rows
    outer_gate_rows, inner_gate_rows, value_rows = tuple(
        (jnp.dot(columns, piece, preferred_element_type=jnp.float32) for piece in pieces)
    )
    outer_gate_rows = outer_gate_rows.astype(jnp.bfloat16)
    inner_gate_rows = inner_gate_rows.astype(jnp.bfloat16)
    value_rows = value_rows.astype(jnp.bfloat16)
    taps = lax.dynamic_slice_in_dim(filter_taps_weight, index * local_width, local_width, 1)
    inner_product_rows = inner_gate_rows.astype(jnp.float32) * value_rows.astype(jnp.float32)
    mixed = (outer_gate_rows.astype(jnp.float32) * causal_mix(inner_product_rows, taps)).astype(
        jnp.bfloat16
    )
    partial_value = settle(
        jnp.dot(
            mixed,
            lax.all_gather(mixer_output_weight, "fs", axis=1, tiled=True),
            preferred_element_type=jnp.float32,
        )
    )
    total = lax.psum(partial_value.astype(jnp.bfloat16), "tp").astype(jnp.float32)
    resid = (tokens.astype(jnp.float32) + total).astype(jnp.bfloat16)
    second = rms_norm(resid, feedforward_norm_gain)
    columns = second
    lifted = jnp.maximum(
        jnp.dot(
            columns,
            lax.all_gather(up_projection_weight, "fs", axis=0, tiled=True),
            preferred_element_type=jnp.float32,
        ),
        0.0,
    )
    hidden = (lifted * lifted).astype(jnp.bfloat16)
    down = jnp.dot(
        hidden,
        lax.all_gather(down_projection_weight, "fs", axis=1, tiled=True),
        preferred_element_type=jnp.float32,
    )
    total_down = lax.psum(settle(down).astype(jnp.bfloat16), "tp").astype(jnp.float32)
    return (resid.astype(jnp.float32) + total_down).astype(jnp.bfloat16)


def solution(mesh):
    return jax.shard_map(
        on_device,
        mesh=mesh,
        in_specs=(
            P("fs", None),
            P(),
            P("fs", "tp"),
            P("fs", "tp"),
            P("fs", "tp"),
            P(),
            P("tp", "fs"),
            P(),
            P("fs", "tp"),
            P("tp", "fs"),
        ),
        out_specs=P("fs", None),
        check_vma=False,
    )
```

profile of v0, /device:TPU:0, one launch (start us, length us, event | category | flops | bytes accessed | tf_op | source)
XLA Modules:
  0.0 859.7 jit_solution(13592114975854171140)
XLA Ops:
  6.5 0.7 all-gather.9.cloned.1.call-update
  7.3 0.0 all-gather.11.cloned.1.call-start
  7.3 0.7 all-gather.11.cloned.1.call-update
  8.0 0.0 all-gather.13.cloned.1.call-start
  8.1 0.7 all-gather.13.cloned.1.call-update
  8.7 0.0 all-gather.7.cloned.1.call-start
  8.8 0.5 all-gather.7.cloned.1.call-update
  9.3 0.0 all-reduce.4.cloned.1.call-start
  9.4 0.9 constant_dynamic-slice_fusion
  10.3 1.8 fusion.1
  12.1 0.0 copy-start.2
  12.1 76.3 %all-gather.9.cloned.1.call-done = bf16[2048,1024]{1,0:T(8,128)(2,1)} async-done(((bf16[128,1024]{1,0:T(8,128)(2,1)}), bf16[2048,1024]{1,0:T(8,128)(2,1)}) %all-gather.9.cloned.1.call-update) | async-done | bytes 4194320 | tf_op jit(solution)/shard_map/all_gather | solution.py:45
  88.4 4.5 convolution_convert_fusion.2
  93.0 72.5 %all-gather.11.cloned.1.call-done = bf16[2048,1024]{1,0:T(8,128)(2,1)} async-done(((bf16[128,1024]{1,0:T(8,128)(2,1)}), bf16[2048,1024]{1,0:T(8,128)(2,1)}) %all-gather.11.cloned.1.call-update) | async-done | bytes 4194320 | tf_op jit(solution)/shard_map/all_gather | solution.py:46
  165.4 5.2 convert_multiply_fusion.4
  170.6 84.9 %all-gather.13.cloned.1.call-done = bf16[1024,2048]{1,0:T(8,128)(2,1)} async-done(((bf16[1024,128]{1,0:T(8,128)(2,1)}), bf16[1024,2048]{1,0:T(8,128)(2,1)}) %all-gather.13.cloned.1.call-update) | async-done | bytes 4194320 | tf_op jit(solution)/shard_map/all_gather | solution.py:63
  255.5 76.4 %all-gather.7.cloned.1.call-done = bf16[2048,1024]{1,0:T(8,128)(2,1)} async-done(((bf16[128,1024]{1,0:T(8,128)(2,1)}), bf16[2048,1024]{1,0:T(8,128)(2,1)}) %all-gather.7.cloned.1.call-update) | async-done | bytes 4194320 | tf_op jit(solution)/shard_map/all_gather | solution.py:44
  331.9 9.9 %convolution_convert_fusion = bf16[384,2048]{1,0:T(8,128)(2,1)} fusion(bf16[1024,2048]{1,0:T(8,128)(2,1)} %all-gather.13.cloned.1.call-done, f32[384,1024]{1,0:T(8,128)} %convert_multiply_fusion.4, bf16[2048,1024]{1,0:T(8,128)(2,1)} %all-gather.7.cloned.1.call-done, f32[1024]{0:T(1024)S(1)} %bitcast.11, f32[1024]{0:T(1024)S(1)} %bitcast.10, ...), kind=kOutput, calls=%fused_computation.18 | convolution fusion | flops 3228696576 | bytes 13129216 | tf_op jit(solution)/shard_map/dot_general | solution.py:61
  341.8 0.0 all-reduce.4.cloned.1.call-update
  341.8 0.0 all-gather.15.cloned.1.call-start
  341.9 0.5 all-gather.15.cloned.1.call-update
  342.4 0.0 all-gather.17.cloned.1.call-start
  342.5 0.7 all-gather.17.cloned.1.call-update
  343.2 0.2 all-reduce.6.cloned.1.call-start
  343.4 17.6 %all-reduce.4.cloned.1.call-done = bf16[384,2048]{1,0:T(8,128)(2,1)} async-done(((bf16[384,2048]{1,0:T(8,128)(2,1)}), bf16[384,2048]{1,0:T(8,128)(2,1)}) %all-reduce.4.cloned.1.call-update) | async-done | bytes 1572880 | tf_op jit(solution)/shard_map/psum | solution.py:67
  361.0 2.1 fusion.5
  363.1 192.7 %all-gather.15.cloned.1.call-done = bf16[2048,4096]{1,0:T(8,128)(2,1)} async-done(((bf16[128,4096]{1,0:T(8,128)(2,1)}), bf16[2048,4096]{1,0:T(8,128)(2,1)}) %all-gather.15.cloned.1.call-update) | async-done | bytes 16777232 | tf_op jit(solution)/shard_map/all_gather | solution.py:74
  555.8 250.0 %all-gather.17.cloned.1.call-done = bf16[4096,2048]{1,0:T(8,128)(2,1)} async-done(((bf16[4096,128]{1,0:T(8,128)(2,1)}), bf16[4096,2048]{1,0:T(8,128)(2,1)}) %all-gather.17.cloned.1.call-update) | async-done | bytes 16777232 | tf_op jit(solution)/shard_map/all_gather | solution.py:82
  805.8 24.9 %fusion.10 = bf16[384,2048]{1,0:T(8,128)(2,1)} fusion(bf16[4096,2048]{1,0:T(8,128)(2,1)} %all-gather.17.cloned.1.call-done, bf16[2048,4096]{1,0:T(8,128)(2,1)} %all-gather.15.cloned.1.call-done, f32[2048]{0:T(1024)S(1)} %copy-done.3, f32[384]{0:T(512)S(1)} %add_rsqrt_fusion, bf16[384,2048]{1,0:T(8,128)(2,1)S(1)} %copy-done, bf16[384,2048]{1,0:T(8,128)(2,1)S(1)} %copy-done.1), kind=kOutput, calls=%fused_computation.17 | convolution fusion | flops 12896698368 | bytes 38282752 | tf_op jit(solution)/shard_map/dot_general | solution.py:80
  830.8 0.0 all-reduce.6.cloned.1.call-update
  830.8 18.7 %all-reduce.6.cloned.1.call-done = bf16[384,2048]{1,0:T(8,128)(2,1)} async-done(((bf16[384,2048]{1,0:T(8,128)(2,1)}), bf16[384,2048]{1,0:T(8,128)(2,1)}) %all-reduce.6.cloned.1.call-update) | async-done | bytes 1572880 | tf_op jit(solution)/shard_map/psum | solution.py:85
  849.5 3.4 fusion.8
  (10 shorter events, 0.0 us)
Async XLA Ops:
  6.5 81.9 %all-gather.9.cloned.1.call-start = ((), (), s32[]{:S(2)}) async-start(), calls=%async_computation.1 | async-start | bytes 4456448 | tf_op jit(solution)/shard_map/all_gather | solution.py:45
  7.3 158.2 %all-gather.11.cloned.1.call-start = ((), (), s32[]{:S(2)}) async-start(), calls=%async_computation.2 | async-start | bytes 4456448 | tf_op jit(solution)/shard_map/all_gather | solution.py:46
  8.0 247.5 %all-gather.13.cloned.1.call-start = ((), (), s32[]{:S(2)}) async-start(), calls=%async_computation.3 | async-start | bytes 4456448 | tf_op jit(solution)/shard_map/all_gather | solution.py:63
  8.7 323.2 %all-gather.7.cloned.1.call-start = ((), (), s32[]{:S(2)}) async-start(), calls=%async_computation | async-start | bytes 4456448 | tf_op jit(solution)/shard_map/all_gather | solution.py:44
  9.3 351.6 %all-reduce.4.cloned.1.call-start = ((), (), s32[]{:S(2)}) async-start(), calls=%async_computation.4 | async-start | bytes 3145728 | tf_op jit(solution)/shard_map/psum | solution.py:67
  12.1 153.3 %copy-start = (bf16[384,2048]{1,0:T(8,128)(2,1)S(1)}, bf16[384,2048]{1,0:T(8,128)(2,1)}, u32[]{:S(2)}) copy-start(bf16[384,2048]{1,0:T(8,128)(2,1)} %param.10) | copy-start | bytes 4718596
  12.1 153.3 %copy-start.2 = (f32[2048]{0:T(1024)S(1)}, f32[2048]{0:T(1024)}, u32[]{:S(2)}) copy-start(f32[2048]{0:T(1024)} %param.11) | copy-start | bytes 24580
  341.8 464.0 %copy-start.3 = (f32[2048]{0:T(1024)S(1)}, f32[2048]{0:T(1024)}, u32[]{:S(2)}) copy-start(f32[2048]{0:T(1024)} %param.17) | copy-start | bytes 24580
  341.8 214.0 %all-gather.15.cloned.1.call-start = ((), (), s32[]{:S(2)}) async-start(), calls=%async_computation.5 | async-start | bytes 17825792 | tf_op jit(solution)/shard_map/all_gather | solution.py:74
  342.4 463.4 %all-gather.17.cloned.1.call-start = ((), (), s32[]{:S(2)}) async-start(), calls=%async_computation.6 | async-start | bytes 17825792 | tf_op jit(solution)/shard_map/all_gather | solution.py:82
  343.2 506.3 %all-reduce.6.cloned.1.call-start = ((), (), s32[]{:S(2)}) async-start(), calls=%async_computation.7 | async-start | bytes 3145728 | tf_op jit(solution)/shard_map/psum | solution.py:85
  361.0 444.9 %copy-start.1 = (bf16[384,2048]{1,0:T(8,128)(2,1)S(1)}, bf16[384,2048]{1,0:T(8,128)(2,1)}, u32[]{:S(2)}) copy-start(bf16[384,2048]{1,0:T(8,128)(2,1)} %all-reduce.4.cloned.1.call-done) | copy-start | bytes 4718596
Sparse Core Ops, SparseCore 0:
  10.1 78.3 all-gather.8
  91.2 74.1 all-gather.10
  168.1 87.3 all-gather.12
  258.1 73.7 all-gather.6
  342.0 18.9 all-reduce.3
  363.6 192.1 all-gather.14
  558.5 247.2 all-gather.16
  830.9 18.5 all-reduce.5
where the time goes:
time: 860 us
  waiting for transfers between devices  793 us (92%)
  matrix products  44.5 us (5%)
  between operations  13.5 us (2%)
    all_gather x1, waiting for transfers between devices, on_device(): lax.all_gather(down_projection_weight, 'fs', axis=1, tiled=True)  250 us
    all_gather x1, waiting for transfers between devices, on_device(): lax.all_gather(up_projection_weight, 'fs', axis=0, tiled=True)  193 us
    all_gather x1, waiting for transfers between devices, on_device(): lax.all_gather(mixer_output_weight, 'fs', axis=1, tiled=True)  84.9 us
    all_gather x1, waiting for transfers between devices, on_device(): lax.all_gather(outer_gate_weight, 'fs', axis=0, tiled=True)  76.4 us
    all_gather x1, waiting for transfers between devices, on_device(): lax.all_gather(inner_gate_weight, 'fs', axis=0, tiled=True)  76.3 us
    all_gather x1, waiting for transfers between devices, on_device(): lax.all_gather(value_projection_weight, 'fs', axis=0, tiled=True)  72.5 us
    dot_general x1, matrix products, on_device(): jnp.dot(hidden, lax.all_gather(down_projection_weight, 'fs', axis=1, tile...  24.9 us
    psum x1, waiting for transfers between devices, on_device(): lax.psum(settle(down).astype(jnp.bfloat16), 'tp').astype(jnp.float32)  18.7 us
  transfers between devices with their start and end apart: 8, of which 8 were waited for; matrix products, arithmetic and copies ran while one was open for 2% of the time, Pallas kernels for 0%

commit v1 on v0

--- a/solution.py
+++ b/solution.py
@@ -79,7 +79,7 @@
     hidden = (lifted * lifted).astype(jnp.bfloat16)
     down = jnp.dot(
         hidden,
-        lax.all_gather(down_projection_weight, "fs", axis=1, tiled=True),
+        jnp.concatenate(lax.all_gather(down_projection_weight, "fs"), axis=1),
         preferred_element_type=jnp.float32,
     )
     total_down = lax.psum(settle(down).astype(jnp.bfloat16), "tp").astype(jnp.float32)

time: 860 us -> 796 us (0.926)
  waiting for transfers between devices: 793 us -> 714 us
  local copies, waits for them, and re-layouts: 0.93 us -> 22.6 us
    all_gather x1, waiting for transfers between devices: 250 us -> 193 us  [on_device(): lax.all_gather(down_projection_weight, 'fs')]
    all_gather x1, waiting for transfers between devices: 193 us -> 170 us  [on_device(): lax.all_gather(up_projection_weight, 'fs', axis=0, tiled=True)]
    reshape x0 -> x1, local copies, waits for them, and re-layouts: none -> 21.6 us  [on_device(): jnp.concatenate(lax.all_gather(down_projection_weight, 'fs'), axis=1)]
  transfers between devices with their start and end apart: 8 -> 8, of which waited for: 8 -> 8; matrix products, arithmetic and copies ran while one was open for 2% -> 5% of each run, Pallas kernels for 0% -> 0%
where the time goes in v1:
time: 796 us; the launch traced here: 795 us
  waiting for transfers between devices  714 us (90%)
  matrix products  38.3 us (5%)
  local copies, waits for them, and re-layouts  22.6 us (3%)
  between operations  13.5 us (2%)
    all_gather x1, waiting for transfers between devices, on_device(): lax.all_gather(down_projection_weight, 'fs')  193 us
    all_gather x1, waiting for transfers between devices, on_device(): lax.all_gather(up_projection_weight, 'fs', axis=0, tiled=True)  170 us
    all_gather x1, waiting for transfers between devices, on_device(): lax.all_gather(mixer_output_weight, 'fs', axis=1, tiled=True)  84.9 us
    all_gather x1, waiting for transfers between devices, on_device(): lax.all_gather(outer_gate_weight, 'fs', axis=0, tiled=True)  76.4 us
    all_gather x1, waiting for transfers between devices, on_device(): lax.all_gather(inner_gate_weight, 'fs', axis=0, tiled=True)  76.3 us
    all_gather x1, waiting for transfers between devices, on_device(): lax.all_gather(value_projection_weight, 'fs', axis=0, tiled=True)  72.5 us
    reshape x1, local copies, waits for them, and re-layouts, on_device(): jnp.concatenate(lax.all_gather(down_projection_weight, 'fs'), axis=1)  21.6 us
    dot_general x1, matrix products, on_device(): jnp.dot(hidden, jnp.concatenate(lax.all_gather(down_projection_weight, 'f...  18.8 us
  transfers between devices with their start and end apart: 8, of which 8 were waited for; matrix products, arithmetic and copies ran while one was open for 5% of the time, Pallas kernels for 0%

profile of v1, /device:TPU:0, one launch (start us, length us, event | category | flops | bytes accessed | tf_op | source)
XLA Modules:
  0.0 795.4 jit_solution(6992488844029469271)
XLA Ops:
  6.5 0.7 all-gather.10.cloned.1.call-update
  7.3 0.0 all-gather.12.cloned.1.call-start
  7.3 0.7 all-gather.12.cloned.1.call-update
  8.0 0.0 all-gather.14.cloned.1.call-start
  8.1 0.7 all-gather.14.cloned.1.call-update
  8.7 0.0 all-gather.8.cloned.1.call-start
  8.8 0.5 all-gather.8.cloned.1.call-update
  9.3 0.0 all-reduce.4.cloned.1.call-start
  9.4 0.9 constant_dynamic-slice_fusion
  10.3 1.8 fusion
  12.1 76.3 %all-gather.10.cloned.1.call-done = bf16[2048,1024]{1,0:T(8,128)(2,1)} async-done(((bf16[128,1024]{1,0:T(8,128)(2,1)}), bf16[2048,1024]{1,0:T(8,128)(2,1)}) %all-gather.10.cloned.1.call-update) | async-done | bytes 4194320 | tf_op jit(solution)/shard_map/all_gather | solution.py:45
  88.4 4.5 convolution_convert_fusion.2
  93.0 72.5 %all-gather.12.cloned.1.call-done = bf16[2048,1024]{1,0:T(8,128)(2,1)} async-done(((bf16[128,1024]{1,0:T(8,128)(2,1)}), bf16[2048,1024]{1,0:T(8,128)(2,1)}) %all-gather.12.cloned.1.call-update) | async-done | bytes 4194320 | tf_op jit(solution)/shard_map/all_gather | solution.py:46
  165.4 5.2 convert_multiply_fusion.4
  170.6 84.9 %all-gather.14.cloned.1.call-done = bf16[1024,2048]{1,0:T(8,128)(2,1)} async-done(((bf16[1024,128]{1,0:T(8,128)(2,1)}), bf16[1024,2048]{1,0:T(8,128)(2,1)}) %all-gather.14.cloned.1.call-update) | async-done | bytes 4194320 | tf_op jit(solution)/shard_map/all_gather | solution.py:63
  255.5 76.4 %all-gather.8.cloned.1.call-done = bf16[2048,1024]{1,0:T(8,128)(2,1)} async-done(((bf16[128,1024]{1,0:T(8,128)(2,1)}), bf16[2048,1024]{1,0:T(8,128)(2,1)}) %all-gather.8.cloned.1.call-update) | async-done | bytes 4194320 | tf_op jit(solution)/shard_map/all_gather | solution.py:44
  331.9 9.8 %convolution_convert_fusion = bf16[384,2048]{1,0:T(8,128)(2,1)} fusion(bf16[1024,2048]{1,0:T(8,128)(2,1)} %all-gather.14.cloned.1.call-done, f32[384,1024]{1,0:T(8,128)} %convert_multiply_fusion.4, bf16[2048,1024]{1,0:T(8,128)(2,1)} %all-gather.8.cloned.1.call-done, f32[1024]{0:T(1024)S(1)} %bitcast.17, f32[1024]{0:T(1024)S(1)} %bitcast.16, ...), kind=kOutput, calls=%fused_computation.17 | convolution fusion | flops 3228696576 | bytes 13129216 | tf_op jit(solution)/shard_map/dot_general | solution.py:61
  341.7 0.0 all-reduce.4.cloned.1.call-update
  341.8 0.0 all-gather.18.cloned.1.call-start
  341.8 0.5 all-gather.18.cloned.1.call-update
  342.3 0.0 all-gather.16.cloned.1.call-start
  342.4 0.7 all-gather.16.cloned.1.call-update
  343.1 0.0 all-reduce.6.cloned.1.call-start
  343.1 17.7 %all-reduce.4.cloned.1.call-done = bf16[384,2048]{1,0:T(8,128)(2,1)} async-done(((bf16[384,2048]{1,0:T(8,128)(2,1)}), bf16[384,2048]{1,0:T(8,128)(2,1)}) %all-reduce.4.cloned.1.call-update) | async-done | bytes 1572880 | tf_op jit(solution)/shard_map/psum | solution.py:67
  360.9 2.0 fusion.4
  362.9 192.8 %all-gather.18.cloned.1.call-done = bf16[65536,128]{1,0:T(8,128)(2,1)} async-done(((bf16[4096,128]{1,0:T(8,128)(2,1)}), bf16[65536,128]{1,0:T(8,128)(2,1)}) %all-gather.18.cloned.1.call-update) | async-done | bytes 16777232 | tf_op jit(solution)/shard_map/all_gather | solution.py:82
  555.7 21.6 %copy.11 = bf16[4096,16,128]{0,2,1:T(8,128)(2,1)} copy(bf16[4096,16,128]{2,0,1:T(8,128)(2,1)} %bitcast.13) | data formatting | bytes 33554432 | tf_op jit(solution)/shard_map/reshape | solution.py:82
  577.4 170.3 %all-gather.16.cloned.1.call-done = bf16[2048,4096]{1,0:T(8,128)(2,1)} async-done(((bf16[128,4096]{1,0:T(8,128)(2,1)}), bf16[2048,4096]{1,0:T(8,128)(2,1)}) %all-gather.16.cloned.1.call-update) | async-done | bytes 16777232 | tf_op jit(solution)/shard_map/all_gather | solution.py:74
  747.7 18.8 %fusion.9 = bf16[384,2048]{1,0:T(8,128)(2,1)} fusion(bf16[4096,2048]{0,1:T(8,128)(2,1)} %bitcast.14, bf16[2048,4096]{1,0:T(8,128)(2,1)} %all-gather.16.cloned.1.call-done, f32[2048]{0:T(1024)S(1)} %copy-done.3, f32[384]{0:T(512)S(1)} %add_rsqrt_fusion, bf16[384,2048]{1,0:T(8,128)(2,1)S(1)} %copy-done, bf16[384,2048]{1,0:T(8,128)(2,1)S(1)} %copy-done.1), kind=kOutput, calls=%fused_computation.16 | convolution fusion | flops 12896698368 | bytes 38282752 | tf_op jit(solution)/shard_map/dot_general | solution.py:80
  766.5 0.0 all-reduce.6.cloned.1.call-update
  766.5 18.7 %all-reduce.6.cloned.1.call-done = bf16[384,2048]{1,0:T(8,128)(2,1)} async-done(((bf16[384,2048]{1,0:T(8,128)(2,1)}), bf16[384,2048]{1,0:T(8,128)(2,1)}) %all-reduce.6.cloned.1.call-update) | async-done | bytes 1572880 | tf_op jit(solution)/shard_map/psum | solution.py:85
  785.2 3.4 fusion.7
  (11 shorter events, 0.0 us)
Async XLA Ops:
  6.5 81.9 %all-gather.10.cloned.1.call-start = ((), (), s32[]{:S(2)}) async-start(), calls=%async_computation.1 | async-start | bytes 4456448 | tf_op jit(solution)/shard_map/all_gather | solution.py:45
  7.3 158.2 %all-gather.12.cloned.1.call-start = ((), (), s32[]{:S(2)}) async-start(), calls=%async_computation.2 | async-start | bytes 4456448 | tf_op jit(solution)/shard_map/all_gather | solution.py:46
  8.0 247.5 %all-gather.14.cloned.1.call-start = ((), (), s32[]{:S(2)}) async-start(), calls=%async_computation.3 | async-start | bytes 4456448 | tf_op jit(solution)/shard_map/all_gather | solution.py:63
  8.7 323.2 %all-gather.8.cloned.1.call-start = ((), (), s32[]{:S(2)}) async-start(), calls=%async_computation | async-start | bytes 4456448 | tf_op jit(solution)/shard_map/all_gather | solution.py:44
  9.3 351.6 %all-reduce.4.cloned.1.call-start = ((), (), s32[]{:S(2)}) async-start(), calls=%async_computation.4 | async-start | bytes 3145728 | tf_op jit(solution)/shard_map/psum | solution.py:67
  12.1 153.3 %copy-start = (bf16[384,2048]{1,0:T(8,128)(2,1)S(1)}, bf16[384,2048]{1,0:T(8,128)(2,1)}, u32[]{:S(2)}) copy-start(bf16[384,2048]{1,0:T(8,128)(2,1)} %param.10) | copy-start | bytes 4718596
  12.1 153.3 %copy-start.2 = (f32[2048]{0:T(1024)S(1)}, f32[2048]{0:T(1024)}, u32[]{:S(2)}) copy-start(f32[2048]{0:T(1024)} %param.11) | copy-start | bytes 24580
  341.8 213.9 %all-gather.18.cloned.1.call-start = ((), (), s32[]{:S(2)}) async-start(), calls=%async_computation.7 | async-start | bytes 17825792 | tf_op jit(solution)/shard_map/all_gather | solution.py:82
  342.3 405.4 %all-gather.16.cloned.1.call-start = ((), (), s32[]{:S(2)}) async-start(), calls=%async_computation.5 | async-start | bytes 17825792 | tf_op jit(solution)/shard_map/all_gather | solution.py:74
  343.1 442.1 %all-reduce.6.cloned.1.call-start = ((), (), s32[]{:S(2)}) async-start(), calls=%async_computation.6 | async-start | bytes 3145728 | tf_op jit(solution)/shard_map/psum | solution.py:85
  555.7 192.0 %copy-start.1 = (bf16[384,2048]{1,0:T(8,128)(2,1)S(1)}, bf16[384,2048]{1,0:T(8,128)(2,1)}, u32[]{:S(2)}) copy-start(bf16[384,2048]{1,0:T(8,128)(2,1)} %all-reduce.4.cloned.1.call-done) | copy-start | bytes 4718596
  555.7 192.0 %copy-start.3 = (f32[2048]{0:T(1024)S(1)}, f32[2048]{0:T(1024)}, u32[]{:S(2)}) copy-start(f32[2048]{0:T(1024)} %param.17) | copy-start | bytes 24580
Sparse Core Ops, SparseCore 0:
  10.1 78.3 all-gather.9
  91.2 74.1 all-gather.11
  168.1 87.3 all-gather.13
  258.1 73.7 all-gather.7
  341.9 18.9 all-reduce.3
  363.5 192.1 all-gather.17
  558.5 189.1 all-gather.15
  766.6 18.5 all-reduce.5
